TPU v7x, 32 devices: a whole 2x2x4 slice. The times are simulated.
32 devices in a mesh: kv: 16 (over z, y, x), tp: 2 (over core).
Axes of the slice: x: 2, y: 2, z: 4, core: 2. Of those that a mesh axis runs over, the one named last changes fastest.
Arguments:
- residual_in: bfloat16 [96, 2048], P('kv', 'tp'), may hold values from -36 to 36
- gain_pre: float32 [2048], P('tp'), may hold values from 0.1 to 1.9
- gate_pre: bfloat16 [2048, 5632], P('tp', 'kv'), may hold values from -0.125 to 0.125
- up_pre: bfloat16 [2048, 5632], P('tp', 'kv'), may hold values from -0.125 to 0.125
- down_pre: bfloat16 [5632, 2048], P('kv', 'tp'), may hold values from -0.078125 to 0.078125
- gain_mix: float32 [2048], replicated, may hold values from 0.1 to 1.9
- query_weight: bfloat16 [2048, 2048], P('kv', 'tp'), may hold values from -0.125 to 0.125
- forget_weight: bfloat16 [2048, 2048], P('kv', 'tp'), may hold values from -0.125 to 0.125
- value_weight: bfloat16 [2048, 2048], P('kv', 'tp'), may hold values from -0.125 to 0.125
- outgate_weight: bfloat16 [2048, 2048], P('kv', 'tp'), may hold values from -0.125 to 0.125
- lower_bound: float32 [2048], P('tp'), may hold values from 0.05 to 0.95
- head_gain: float32 [2048], P('tp'), may hold values from 0.1 to 1.9
- out_weight: bfloat16 [2048, 2048], P('tp'), may hold values from -0.125 to 0.125
- gain_post: float32 [2048], P('tp'), may hold values from 0.1 to 1.9
- gate_post: bfloat16 [2048, 5632], P('tp', 'kv'), may hold values from -0.125 to 0.125
- up_post: bfloat16 [2048, 5632], P('tp', 'kv'), may hold values from -0.125 to 0.125
- down_post: bfloat16 [5632, 2048], P('kv', 'tp'), may hold values from -0.078125 to 0.078125
- memory_state: float32 [96, 16, 128, 128], P('kv', 'tp'), may hold values from -4 to 4
Outputs:
- layer_out: bfloat16 [96, 2048], P('kv', 'tp')
- next_state: float32 [96, 16, 128, 128], P('kv', 'tp')
All inputs are finite; a program needn't handle non-finite values.
Results may differ from a plain program's by a relative error of at most 0.014.
Values may be sent and summed in bfloat16 or wider, within the bound.
A program may use at most 64 MiB of HBM per device.

v0:
```python
import jax
import jax.numpy as jnp
from jax import lax
from jax.sharding import PartitionSpec as P

D = 2048
HEAD_DIM = 128


EPSILON = 1e-06


def channel_mixer(row_block, gain_vec, gate_weight, up_weight, down_weight):
    gathered = lax.all_gather(row_block, "kv", axis=0, tiled=True)
    widened = gathered.astype(jnp.float32)
    part_squares = jnp.sum(widened * widened, axis=1)
    scaled = (widened * gain_vec).astype(jnp.bfloat16)
    gate_part = jnp.dot(scaled, gate_weight, preferred_element_type=jnp.float32)
    up_part = jnp.dot(scaled, up_weight, preferred_element_type=jnp.float32)
    gate_share, up_share, square_share = (
        lax.psum_scatter(
            gate_part.astype(jnp.bfloat16), "tp", scatter_dimension=0, tiled=True
        ).astype(jnp.float32),
        lax.psum_scatter(
            up_part.astype(jnp.bfloat16), "tp", scatter_dimension=0, tiled=True
        ).astype(jnp.float32),
        lax.psum_scatter(
            part_squares.astype(jnp.bfloat16), "tp", scatter_dimension=0, tiled=True
        ).astype(jnp.float32),
    )
    share_inverse = lax.rsqrt(square_share / D + EPSILON)[:, None]
    hidden_share = (jax.nn.silu(gate_share * share_inverse) * (up_share * share_inverse)).astype(
        jnp.bfloat16
    )
    hidden = lax.all_gather(hidden_share, "tp", axis=0, tiled=True)
    return lax.psum_scatter(
        jnp.dot(hidden, down_weight, preferred_element_type=jnp.float32),
        "kv",
        scatter_dimension=0,
        tiled=True,
    )


def token_mixer(
    stream_a,
    gain_mix,
    query_weight,
    forget_weight,
    value_weight,
    outgate_weight,
    lower_bound,
    head_gain,
    out_weight,
    memory_state,
):
    full_rows = lax.all_gather(stream_a, "tp", axis=1, tiled=True)
    widened = full_rows.astype(jnp.float32)
    inverse = lax.rsqrt(jnp.mean(widened * widened, axis=1, keepdims=True) + EPSILON)
    scaled = (widened * gain_mix).astype(jnp.bfloat16)
    weights = (query_weight, forget_weight, value_weight, outgate_weight)
    blocks = lax.all_to_all(scaled, "kv", split_axis=1, concat_axis=0, tiled=True)
    joined = jnp.concatenate(weights, axis=1)
    projected = lax.psum_scatter(
        jnp.dot(blocks, joined, preferred_element_type=jnp.float32),
        "kv",
        scatter_dimension=0,
        tiled=True,
    )
    projected = projected * inverse
    seq_rows = scaled.shape[0]
    local_heads = query_weight.shape[1] // HEAD_DIM
    reshaped = projected.reshape(seq_rows, 4, local_heads, HEAD_DIM)
    query_pre = reshaped[:, 0]
    forget_pre = reshaped[:, 1]
    value_pre = reshaped[:, 2]
    outgate_pre = reshaped[:, 3]
    floor_rate = lower_bound.reshape(local_heads, HEAD_DIM)
    log_keep = jnp.logaddexp(
        jnp.log(floor_rate), jnp.log1p(-floor_rate) + jax.nn.log_sigmoid(forget_pre)
    )
    inject = (1.0 - floor_rate) * jax.nn.sigmoid(-forget_pre)
    next_state = (
        jnp.exp(log_keep)[..., None] * memory_state + inject[..., None] * value_pre[:, :, None, :]
    )
    readout = jnp.einsum(
        "bhk,bhkv->bhv", jax.nn.silu(query_pre), next_state, precision=lax.Precision.HIGHEST
    )
    normed = (
        readout
        * lax.rsqrt(jnp.mean(readout * readout, axis=2, keepdims=True) + EPSILON)
        * head_gain.reshape(local_heads, HEAD_DIM)
    )
    mixed_heads = (
        (normed * jax.nn.silu(outgate_pre))
        .reshape(seq_rows, local_heads * HEAD_DIM)
        .astype(jnp.bfloat16)
    )
    partial_out = jnp.dot(mixed_heads, out_weight, preferred_element_type=jnp.float32)
    mixed = lax.psum_scatter(
        partial_out.astype(jnp.bfloat16), "tp", scatter_dimension=1, tiled=True
    ).astype(jnp.float32)
    return (mixed, next_state)


def shards(
    residual_in,
    gain_pre,
    gate_pre,
    up_pre,
    down_pre,
    gain_mix,
    query_weight,
    forget_weight,
    value_weight,
    outgate_weight,
    lower_bound,
    head_gain,
    out_weight,
    gain_post,
    gate_post,
    up_post,
    down_post,
    memory_state,
):
    branch_a = channel_mixer(residual_in, gain_pre, gate_pre, up_pre, down_pre)
    stream_a = (residual_in.astype(jnp.float32) + 0.5 * branch_a).astype(jnp.bfloat16)
    mixed, next_state = token_mixer(
        stream_a,
        gain_mix,
        query_weight,
        forget_weight,
        value_weight,
        outgate_weight,
        lower_bound,
        head_gain,
        out_weight,
        memory_state,
    )
    stream_b = (stream_a.astype(jnp.float32) + mixed).astype(jnp.bfloat16)
    branch_b = channel_mixer(stream_b, gain_post, gate_post, up_post, down_post)
    layer_out = (stream_b.astype(jnp.float32) + 0.5 * branch_b).astype(jnp.bfloat16)
    return (layer_out, next_state)


def solution(mesh):
    in_specs = (
        P("kv", "tp"),
        P("tp"),
        P("tp", "kv"),
        P("tp", "kv"),
        P("kv", "tp"),
        P(),
        P("kv", "tp"),
        P("kv", "tp"),
        P("kv", "tp"),
        P("kv", "tp"),
        P("tp"),
        P("tp"),
        P("tp", None),
        P("tp"),
        P("tp", "kv"),
        P("tp", "kv"),
        P("kv", "tp"),
        P("kv", "tp", None, None),
    )
    out_specs = (P("kv", "tp"), P("kv", "tp", None, None))
    return jax.shard_map(shards, mesh=mesh, in_specs=in_specs, out_specs=out_specs, check_vma=False)
```

profile of v0, /device:TPU:8, one launch (start us, length us, event | category | flops | bytes accessed | tf_op | source)
XLA Modules:
  0.0 351.1 jit_solution(17581845288127005112)
XLA Ops:
  7.3 36.3 %all-gather = bf16[16,6,1024]{2,1,0:T(8,128)(2,1)S(1)} all-gather(bf16[1,6,1024]{2,1,0:T(8,128)(2,1)} %bitcast.90), channel_id=1, replica_groups=mesh['kv'=16,'tp'=2] {'kv'}, dimensions={0}, use_global_device_ids=true | all-gather | bytes 208896 | tf_op jit(solution)/shard_map/all_gather | solution.py:14
  43.7 2.2 convolution_convert_fusion.4
  45.9 2.1 convolution_convert_fusion.3
  48.2 0.6 dynamic-slice
  49.4 2.5 all-reduce
  52.0 4.0 %reduce-scatter.12.cloned.1.call-done = bf16[48,352]{1,0:T(8,128)(2,1)} async-done(((bf16[96,352]{1,0:T(8,128)(2,1)}), bf16[48,352]{1,0:T(8,128)(2,1)}) %reduce-scatter.12.cloned.1.call-update) | async-done | bytes 33808 | tf_op jit(solution)/shard_map/reduce_scatter | solution.py:21
  55.9 11.5 %reduce-scatter.14.cloned.1.call-done = bf16[48,352]{1,0:T(8,128)(2,1)} async-done(((bf16[96,352]{1,0:T(8,128)(2,1)}), bf16[48,352]{1,0:T(8,128)(2,1)}) %reduce-scatter.14.cloned.1.call-update) | async-done | bytes 33808 | tf_op jit(solution)/shard_map/reduce_scatter | solution.py:24
  67.4 0.9 multiply_convert_fusion.3
  68.3 1.9 all_gather.16
  70.5 39.0 %fusion = f32[8,1024]{1,0:T(8,128)S(1)} fusion(f32[96,1024]{1,0:T(8,128)S(1)} %fusion.36), kind=kCustom, calls=%all-reduce-scatter | all-reduce-scatter fusion | flops 131073 | bytes 426496
  109.4 1.9 collective-permute-start.2
  111.4 2.3 collective-permute-start.1
  113.7 2.0 collective-permute-start
  115.8 7.4 %collective-permute-start.3 = (f32[6,1024]{1,0:T(8,128)S(1)}, f32[6,1024]{1,0:T(8,128)S(1)}, u32[]{:S(2)}, u32[]{:S(2)}) collective-permute-start(f32[6,1024]{1,0:T(8,128)S(1)} %slice.20), channel_id=1, source_target_pairs={{0,8},{2,10},{4,12},{6,14},{8,16},{10,18},{12,20},{14,22},{16,24},... | collective-permute-start | bytes 73736
  123.2 0.6 dynamic-slice.12
  124.8 0.4 concatenate.4
  125.3 1.8 all_gather.17
  127.1 0.7 fusion.13
  127.9 7.5 %all-to-all-start = ((bf16[6,16,128]{2,0,1:T(8,128)(2,1)}), bf16[6,16,128]{2,0,1:T(8,128)(2,1)S(1)}, u32[]{:S(2)}, u32[]{:S(2)}) async-start(bf16[6,16,128]{2,0,1:T(8,128)(2,1)} %get-tuple-element.6), calls=%async_computation.2 | async-start | bytes 65536 | tf_op jit(solution)/shard_map/all_to_all | solution.py:61
  135.4 6.0 %all-to-all-done = bf16[6,16,128]{2,0,1:T(8,128)(2,1)S(1)} async-done(((bf16[6,16,128]{2,0,1:T(8,128)(2,1)}), bf16[6,16,128]{2,0,1:T(8,128)(2,1)S(1)}, u32[]{:S(2)}, u32[]{:S(2)}) %all-to-all-start) | async-done | bytes 24608 | tf_op jit(solution)/shard_map/all_to_all | solution.py:61
  141.8 50.6 %fusion.1 = f32[8,4096]{1,0:T(8,128)S(1)} fusion(f32[96,4096]{1,0:T(8,128)S(1)} %fusion.3), kind=kCustom, calls=%all-reduce-scatter.1 | all-reduce-scatter fusion | flops 524289 | bytes 1704448
  192.4 2.5 collective-permute-start.6
  194.9 5.2 %collective-permute-start.5 = (f32[8,4096]{1,0:T(8,128)S(1)}, f32[8,4096]{1,0:T(8,128)S(1)}, u32[]{:S(2)}, u32[]{:S(2)}) collective-permute-start(f32[8,4096]{1,0:T(8,128)S(1)} %fusion.1), channel_id=1, source_target_pairs={{0,4},{2,6},{4,8},{6,10},{8,12},{10,14},{12,16},{14,18},{16,20},{1... | collective-permute-start | bytes 393224
  200.1 2.8 collective-permute-start.4
  202.9 2.5 collective-permute-start.7
  205.4 4.3 %collective-permute-done.7 = f32[6,4096]{1,0:T(8,128)S(1)} collective-permute-done((f32[6,4096]{1,0:T(8,128)S(1)}, f32[6,4096]{1,0:T(8,128)S(1)}, u32[]{:S(2)}, u32[]{:S(2)}) %collective-permute-start.7) | collective-permute-done | bytes 98336
  209.8 0.8 concatenate.5
  210.8 4.0 %multiply_add_fusion = f32[6,8,128,128]{3,2,1,0:T(8,128)S(1)} fusion(f32[6,8,128,128]{3,2,1,0:T(8,128)} %param.35, f32[6,8,128]{2,1,0:T(8,128)S(1)} %slice_bitcast_fusion.1, f32[6,8,128]{2,1,0:T(8,128)S(1)} %get-tuple-element.3, f32[6,8,128]{2,1,0:T(8,128)S(1)} %get-tuple-element.2), kind=kLoop, calls=%fused_computation | loop fusion | flops 2359296 | bytes 6365184 | tf_op jit(solution)/shard_map/add | solution.py:83
  214.8 1.6 copy-done.1
  216.4 2.8 fusion.37
  219.4 1.3 convolution_convert_fusion
  220.7 6.3 %reduce-scatter.16.cloned.1.call-done = bf16[6,1024]{1,0:T(8,128)(2,1)} async-done(((bf16[6,2048]{1,0:T(8,128)(2,1)}), bf16[6,1024]{1,0:T(8,128)(2,1)}) %reduce-scatter.16.cloned.1.call-update) | async-done | bytes 12304 | tf_op jit(solution)/shard_map/reduce_scatter | solution.py:99
  227.1 0.7 fusion.28
  227.8 35.8 %all-gather.1 = bf16[16,6,1024]{2,1,0:T(8,128)(2,1)S(1)} all-gather(bf16[1,6,1024]{2,1,0:T(8,128)(2,1)S(1)} %fusion.28), channel_id=1, replica_groups=mesh['kv'=16,'tp'=2] {'kv'}, dimensions={0}, use_global_device_ids=true | all-gather | bytes 208896 | tf_op jit(solution)/shard_map/all_gather | solution.py:14
  263.6 1.7 convolution_convert_fusion.2
  265.4 1.7 convolution_convert_fusion.1
  267.2 2.5 all-reduce.3
  269.7 5.7 %reduce-scatter.18.cloned.1.call-done = bf16[48,352]{1,0:T(8,128)(2,1)} async-done(((bf16[96,352]{1,0:T(8,128)(2,1)}), bf16[48,352]{1,0:T(8,128)(2,1)}) %reduce-scatter.18.cloned.1.call-update) | async-done | bytes 33808 | tf_op jit(solution)/shard_map/reduce_scatter | solution.py:21
  275.4 10.7 %reduce-scatter.20.cloned.1.call-done = bf16[48,352]{1,0:T(8,128)(2,1)} async-done(((bf16[96,352]{1,0:T(8,128)(2,1)}), bf16[48,352]{1,0:T(8,128)(2,1)}) %reduce-scatter.20.cloned.1.call-update) | async-done | bytes 33808 | tf_op jit(solution)/shard_map/reduce_scatter | solution.py:24
  286.1 0.9 multiply_convert_fusion.2
  287.0 1.9 all_gather.19
  289.2 39.0 %fusion.2 = f32[8,1024]{1,0:T(8,128)S(1)} fusion(f32[96,1024]{1,0:T(8,128)S(1)} %fusion.38), kind=kCustom, calls=%all-reduce-scatter.2 | all-reduce-scatter fusion | flops 131073 | bytes 426496
  328.1 1.9 collective-permute-start.10
  330.1 2.3 collective-permute-start.9
  332.4 2.1 collective-permute-start.8
  334.5 7.4 %collective-permute-start.11 = (f32[6,1024]{1,0:T(8,128)S(1)}, f32[6,1024]{1,0:T(8,128)S(1)}, u32[]{:S(2)}, u32[]{:S(2)}) collective-permute-start(f32[6,1024]{1,0:T(8,128)S(1)} %slice.22), channel_id=1, source_target_pairs={{0,8},{2,10},{4,12},{6,14},{8,16},{10,18},{12,20},{14,22},{16,24},... | collective-permute-start | bytes 73736
  341.9 1.6 collective-permute-done.11
  344.0 0.6 fusion.16
  (77 shorter events, 3.0 us)
Async XLA Ops:
  7.2 63.0 %copy-start = (bf16[352,1024]{1,0:T(8,128)(2,1)S(1)}, bf16[352,1024]{1,0:T(8,128)(2,1)}, u32[]{:S(2)}) copy-start(bf16[352,1024]{1,0:T(8,128)(2,1)} %param.22) | copy-start | bytes 2162692
  7.2 41.0 %copy-start.16 = (u32[32]{0:T(128)S(1)}, u32[32]{0:T(128)}, u32[]{:S(2)}) copy-start(u32[32]{0:T(128)} %constant.33) | copy-start | bytes 388
  7.2 116.0 %copy-start.11 = (u32[32]{0:T(128)S(1)}, u32[32]{0:T(128)}, u32[]{:S(2)}) copy-start(u32[32]{0:T(128)} %constant.37) | copy-start | bytes 388
  7.2 118.0 %copy-start.6 = (bf16[6,1024]{1,0:T(8,128)(2,1)S(1)}, bf16[6,1024]{1,0:T(8,128)(2,1)}, u32[]{:S(2)}) copy-start(bf16[6,1024]{1,0:T(8,128)(2,1)} %param.18) | copy-start | bytes 36868
  7.2 119.9 %copy-start.8 = (f32[2048]{0:T(1024)S(1)}, f32[2048]{0:T(1024)}, u32[]{:S(2)}) copy-start(f32[2048]{0:T(1024)} %param.23) | copy-start | bytes 24580
  7.2 48.7 %reduce-scatter.12.cloned.1.call-start = ((), (), s32[]{:S(2)}) async-start(), calls=%async_computation.6 | async-start | bytes 110592 | tf_op jit(solution)/shard_map/reduce_scatter | solution.py:21
  7.3 128.1 %copy-start.10 = (f32[1024]{0:T(1024)S(1)}, f32[1024]{0:T(1024)}, u32[]{:S(2)}) copy-start(f32[1024]{0:T(1024)} %param.28) | copy-start | bytes 12292
  43.6 97.9 %copy-start.12 = (bf16[128,1024]{1,0:T(8,128)(2,1)S(1)}, bf16[128,1024]{1,0:T(8,128)(2,1)}, u32[]{:S(2)}) copy-start(bf16[128,1024]{1,0:T(8,128)(2,1)} %param.27) | copy-start | bytes 786436
  43.6 97.9 %copy-start.13 = (bf16[128,1024]{1,0:T(8,128)(2,1)S(1)}, bf16[128,1024]{1,0:T(8,128)(2,1)}, u32[]{:S(2)}) copy-start(bf16[128,1024]{1,0:T(8,128)(2,1)} %param.26) | copy-start | bytes 786436
  43.6 97.9 %copy-start.14 = (bf16[128,1024]{1,0:T(8,128)(2,1)S(1)}, bf16[128,1024]{1,0:T(8,128)(2,1)}, u32[]{:S(2)}) copy-start(bf16[128,1024]{1,0:T(8,128)(2,1)} %param.25) | copy-start | bytes 786436
  43.6 97.9 %copy-start.15 = (bf16[128,1024]{1,0:T(8,128)(2,1)S(1)}, bf16[128,1024]{1,0:T(8,128)(2,1)}, u32[]{:S(2)}) copy-start(bf16[128,1024]{1,0:T(8,128)(2,1)} %param.24) | copy-start | bytes 786436
  45.9 21.6 %reduce-scatter.14.cloned.1.call-start = ((), (), s32[]{:S(2)}) async-start(), calls=%async_computation.7 | async-start | bytes 110592 | tf_op jit(solution)/shard_map/reduce_scatter | solution.py:24
  109.4 15.3 %collective-permute-start.2 = (f32[8,1024]{1,0:T(8,128)S(1)}, f32[8,1024]{1,0:T(8,128)S(1)}, u32[]{:S(2)}, u32[]{:S(2)}) collective-permute-start(f32[8,1024]{1,0:T(8,128)S(1)} %fusion), channel_id=1, source_target_pairs={{0,6},{2,8},{4,10},{6,12},{8,14},{10,16},{12,18},{14,20},{16,22},{... | collective-permute-start | bytes 98312
  111.4 13.4 %collective-permute-start.1 = (f32[8,1024]{1,0:T(8,128)S(1)}, f32[8,1024]{1,0:T(8,128)S(1)}, u32[]{:S(2)}, u32[]{:S(2)}) collective-permute-start(f32[8,1024]{1,0:T(8,128)S(1)} %fusion), channel_id=1, source_target_pairs={{0,4},{2,6},{4,8},{6,10},{8,12},{10,14},{12,16},{14,18},{16,20},{1... | collective-permute-start | bytes 98312
  113.7 11.1 %collective-permute-start = (f32[8,1024]{1,0:T(8,128)S(1)}, f32[8,1024]{1,0:T(8,128)S(1)}, u32[]{:S(2)}, u32[]{:S(2)}) collective-permute-start(f32[8,1024]{1,0:T(8,128)S(1)} %fusion), channel_id=1, source_target_pairs={{0,2},{2,4},{4,6},{6,8},{8,10},{10,12},{12,14},{14,16},{16,18},{18... | collective-permute-start | bytes 98312
  115.8 9.0 %collective-permute-start.3 = (f32[6,1024]{1,0:T(8,128)S(1)}, f32[6,1024]{1,0:T(8,128)S(1)}, u32[]{:S(2)}, u32[]{:S(2)}) collective-permute-start(f32[6,1024]{1,0:T(8,128)S(1)} %slice.20), channel_id=1, source_target_pairs={{0,8},{2,10},{4,12},{6,14},{8,16},{10,18},{12,20},{14,22},{16,24},... | collective-permute-start | bytes 73736
  127.9 13.6 %all-to-all-start = ((bf16[6,16,128]{2,0,1:T(8,128)(2,1)}), bf16[6,16,128]{2,0,1:T(8,128)(2,1)S(1)}, u32[]{:S(2)}, u32[]{:S(2)}) async-start(bf16[6,16,128]{2,0,1:T(8,128)(2,1)} %get-tuple-element.6), calls=%async_computation.2 | async-start | bytes 65536 | tf_op jit(solution)/shard_map/all_to_all | solution.py:61
  135.3 91.7 %reduce-scatter.16.cloned.1.call-start = ((), (), s32[]{:S(2)}) async-start(), calls=%async_computation.8 | async-start | bytes 49152 | tf_op jit(solution)/shard_map/reduce_scatter | solution.py:99
  192.4 17.3 %collective-permute-start.6 = (f32[8,4096]{1,0:T(8,128)S(1)}, f32[8,4096]{1,0:T(8,128)S(1)}, u32[]{:S(2)}, u32[]{:S(2)}) collective-permute-start(f32[8,4096]{1,0:T(8,128)S(1)} %fusion.1), channel_id=1, source_target_pairs={{0,6},{2,8},{4,10},{6,12},{8,14},{10,16},{12,18},{14,20},{16,22},{... | collective-permute-start | bytes 393224
  194.9 14.9 %collective-permute-start.5 = (f32[8,4096]{1,0:T(8,128)S(1)}, f32[8,4096]{1,0:T(8,128)S(1)}, u32[]{:S(2)}, u32[]{:S(2)}) collective-permute-start(f32[8,4096]{1,0:T(8,128)S(1)} %fusion.1), channel_id=1, source_target_pairs={{0,4},{2,6},{4,8},{6,10},{8,12},{10,14},{12,16},{14,18},{16,20},{1... | collective-permute-start | bytes 393224
  200.1 9.7 %collective-permute-start.4 = (f32[8,4096]{1,0:T(8,128)S(1)}, f32[8,4096]{1,0:T(8,128)S(1)}, u32[]{:S(2)}, u32[]{:S(2)}) collective-permute-start(f32[8,4096]{1,0:T(8,128)S(1)} %fusion.1), channel_id=1, source_target_pairs={{0,2},{2,4},{4,6},{6,8},{8,10},{10,12},{12,14},{14,16},{16,18},{18... | collective-permute-start | bytes 393224
  202.9 6.9 %collective-permute-start.7 = (f32[6,4096]{1,0:T(8,128)S(1)}, f32[6,4096]{1,0:T(8,128)S(1)}, u32[]{:S(2)}, u32[]{:S(2)}) collective-permute-start(f32[6,4096]{1,0:T(8,128)S(1)} %slice.21), channel_id=1, source_target_pairs={{0,8},{2,10},{4,12},{6,14},{8,16},{10,18},{12,20},{14,22},{16,24},... | collective-permute-start | bytes 294920
  210.7 8.6 %copy-start.2 = (bf16[1024,2048]{1,0:T(8,128)(2,1)S(1)}, bf16[1024,2048]{1,0:T(8,128)(2,1)}, u32[]{:S(2)}) copy-start(bf16[1024,2048]{1,0:T(8,128)(2,1)} %param.30) | copy-start | bytes 12582916
  214.7 1.7 copy-start.1
  214.8 4.5 %copy-start.9 = (f32[1024]{0:T(1024)S(1)}, f32[1024]{0:T(1024)}, u32[]{:S(2)}) copy-start(f32[1024]{0:T(1024)} %param.29) | copy-start | bytes 12292
  219.2 44.4 %copy-start.3 = (bf16[1024,352]{0,1:T(8,128)(2,1)S(1)}, bf16[1024,352]{0,1:T(8,128)(2,1)}, u32[]{:S(2)}) copy-start(bf16[1024,352]{0,1:T(8,128)(2,1)} %param.32) | copy-start | bytes 2162692
  219.4 46.0 %copy-start.4 = (bf16[1024,352]{0,1:T(8,128)(2,1)S(1)}, bf16[1024,352]{0,1:T(8,128)(2,1)}, u32[]{:S(2)}) copy-start(bf16[1024,352]{0,1:T(8,128)(2,1)} %param.33) | copy-start | bytes 2162692
  220.6 68.3 %copy-start.5 = (bf16[352,1024]{1,0:T(8,128)(2,1)S(1)}, bf16[352,1024]{1,0:T(8,128)(2,1)}, u32[]{:S(2)}) copy-start(bf16[352,1024]{1,0:T(8,128)(2,1)} %param.34) | copy-start | bytes 2162692
  220.7 54.7 %reduce-scatter.18.cloned.1.call-start = ((), (), s32[]{:S(2)}) async-start(), calls=%async_computation.9 | async-start | bytes 110592 | tf_op jit(solution)/shard_map/reduce_scatter | solution.py:21
  263.6 80.3 %copy-start.7 = (bf16[6,1024]{1,0:T(8,128)(2,1)S(1)}, bf16[6,1024]{1,0:T(8,128)(2,1)}, u32[]{:S(2)}) copy-start(bf16[6,1024]{1,0:T(8,128)(2,1)} %reduce-scatter.16.cloned.1.call-done) | copy-start | bytes 36868
  265.3 20.8 %reduce-scatter.20.cloned.1.call-start = ((), (), s32[]{:S(2)}) async-start(), calls=%async_computation.10 | async-start | bytes 110592 | tf_op jit(solution)/shard_map/reduce_scatter | solution.py:24
  328.1 15.3 %collective-permute-start.10 = (f32[8,1024]{1,0:T(8,128)S(1)}, f32[8,1024]{1,0:T(8,128)S(1)}, u32[]{:S(2)}, u32[]{:S(2)}) collective-permute-start(f32[8,1024]{1,0:T(8,128)S(1)} %fusion.2), channel_id=1, source_target_pairs={{0,6},{2,8},{4,10},{6,12},{8,14},{10,16},{12,18},{14,20},{16,22},{... | collective-permute-start | bytes 98312
  330.1 13.4 %collective-permute-start.9 = (f32[8,1024]{1,0:T(8,128)S(1)}, f32[8,1024]{1,0:T(8,128)S(1)}, u32[]{:S(2)}, u32[]{:S(2)}) collective-permute-start(f32[8,1024]{1,0:T(8,128)S(1)} %fusion.2), channel_id=1, source_target_pairs={{0,4},{2,6},{4,8},{6,10},{8,12},{10,14},{12,16},{14,18},{16,20},{1... | collective-permute-start | bytes 98312
  332.4 11.1 %collective-permute-start.8 = (f32[8,1024]{1,0:T(8,128)S(1)}, f32[8,1024]{1,0:T(8,128)S(1)}, u32[]{:S(2)}, u32[]{:S(2)}) collective-permute-start(f32[8,1024]{1,0:T(8,128)S(1)} %fusion.2), channel_id=1, source_target_pairs={{0,2},{2,4},{4,6},{6,8},{8,10},{10,12},{12,14},{14,16},{16,18},{18... | collective-permute-start | bytes 98312
  334.5 9.0 %collective-permute-start.11 = (f32[6,1024]{1,0:T(8,128)S(1)}, f32[6,1024]{1,0:T(8,128)S(1)}, u32[]{:S(2)}, u32[]{:S(2)}) collective-permute-start(f32[6,1024]{1,0:T(8,128)S(1)} %slice.22), channel_id=1, source_target_pairs={{0,8},{2,10},{4,12},{6,14},{8,16},{10,18},{12,20},{14,22},{16,24},... | collective-permute-start | bytes 73736
Sparse Core Ops, SparseCore 0:
  46.0 9.9 reduce-scatter.11
  58.7 8.6 reduce-scatter.13
  220.8 6.2 reduce-scatter.15
  265.4 9.9 reduce-scatter.17
  277.4 8.6 reduce-scatter.19
where the time goes:
time: 354 us; the launch traced here: 351 us
  blocking collectives  211 us (60%)
  waiting for transfers between devices  50.5 us (14%)
  starting transfers between devices  48.1 us (14%)
  between operations  15.6 us (4%)
  matrix products  12.6 us (4%)
  other arithmetic  8.58 us (2%)
  local copies, waits for them, and re-layouts  4.76 us (1%)
    unnamed x5, blocking collectives  133 us
    all_gather x2, blocking collectives, channel_mixer(): gathered = lax.all_gather(row_block, 'kv', axis=0, tiled=True)  72 us
    unnamed x12, starting transfers between devices  40.4 us
    reduce_scatter x2, waiting for transfers between devices, channel_mixer(): lax.psum_scatter(up_part.astype(jnp.bfloat16), 'tp', scatter_dimension=0,...  22.2 us
    reduce_scatter x2, waiting for transfers between devices, channel_mixer(): lax.psum_scatter(gate_part.astype(jnp.bfloat16), 'tp', scatter_dimension=...  9.62 us
    all_to_all x1, starting transfers between devices, token_mixer(): lax.all_to_all(scaled, 'kv', split_axis=1, concat_axis=0, tiled=True)  7.47 us
  transfers between devices with their start and end apart: 18, of which 9 were waited for; matrix products, arithmetic and copies ran while one was open for 2% of the time, Pallas kernels for 0%

commit v1 on v0

--- a/solution.py
+++ b/solution.py
@@ -1,6 +1,10 @@
+import functools
+
 import jax
 import jax.numpy as jnp
 from jax import lax
+from jax.experimental import pallas as pl
+from jax.experimental.pallas import tpu as pltpu
 from jax.sharding import PartitionSpec as P
 
 D = 2048
@@ -142,7 +146,430 @@
     return (layer_out, next_state)
 
 
+ROW_PAD = 8
+GATHER_A, SCATTER_A, COLUMNS, PROJECT, GATHER_B, SCATTER_B = 0, 1, 2, 3, 7, 8
+KV_EXCHANGES = 9
+
+
+def fused_layer(
+    n_kv,
+    residual_ref,
+    gain_pre_ref,
+    gain_mix_ref,
+    lower_ref,
+    head_gain_ref,
+    gain_post_ref,
+    gate_pre_hbm,
+    up_pre_hbm,
+    down_pre_hbm,
+    query_hbm,
+    forget_hbm,
+    value_hbm,
+    outgate_hbm,
+    out_hbm,
+    gate_post_hbm,
+    up_post_hbm,
+    down_post_hbm,
+    state_hbm,
+    layer_ref,
+    next_hbm,
+    gate_pre,
+    up_pre,
+    down_pre,
+    proj_weights,
+    out_weight,
+    gate_post,
+    up_post,
+    down_post,
+    state,
+    gather_a,
+    gather_b,
+    partial_a,
+    partial_b,
+    landed_a,
+    landed_b,
+    gate_up_out,
+    gate_up_in,
+    squares_out,
+    squares_in,
+    stream_out,
+    stream_in,
+    column_out,
+    column_in,
+    proj_out,
+    proj_in,
+    mixed_out,
+    mixed_in,
+    residual_pad,
+    keep_t,
+    inject_t,
+    query_t,
+    value_rows,
+    readout,
+    load_sem,
+    store_sem,
+    kv_send,
+    kv_recv,
+    tp_send,
+    tp_recv,
+):
+    me = lax.axis_index("kv")
+    core = lax.axis_index("tp")
+    rows, width = residual_ref.shape
+    model = 2 * width
+    f32, bf16 = jnp.float32, jnp.bfloat16
+
+    def load(index, source, target):
+        return pltpu.make_async_copy(source, target, load_sem.at[index])
+
+    loads = [
+        load(0, gate_pre_hbm, gate_pre),
+        load(1, up_pre_hbm, up_pre),
+        load(2, down_pre_hbm, down_pre),
+        load(3, forget_hbm, proj_weights.at[0]),
+        load(4, value_hbm, proj_weights.at[1]),
+        load(5, query_hbm, proj_weights.at[2]),
+        load(6, outgate_hbm, proj_weights.at[3]),
+        load(7, state_hbm, state),
+        load(8, out_hbm, out_weight),
+        load(9, gate_post_hbm, gate_post),
+        load(10, up_post_hbm, up_post),
+        load(11, down_post_hbm, down_post),
+    ]
+    for copy in loads:
+        copy.start()
+
+    residual_pad[...] = jnp.zeros_like(residual_pad)
+    residual_pad[0:rows, :] = residual_ref[...].astype(f32)
+    gather_a[me] = residual_pad[...].astype(bf16)
+    readout[...] = jnp.zeros_like(readout)
+
+    barrier = pltpu.get_barrier_semaphore()
+
+    def greet(step, carry):
+        pl.semaphore_signal(
+            barrier,
+            inc=1,
+            device_id={"kv": lax.rem(me + step, n_kv)},
+            device_id_type=pl.DeviceIdType.MESH,
+        )
+        return carry
+
+    lax.fori_loop(1, n_kv, greet, 0)
+    pl.semaphore_signal(
+        barrier, inc=1, device_id={"tp": 1 - core}, device_id_type=pl.DeviceIdType.MESH
+    )
+    pl.semaphore_wait(barrier, n_kv)
+
+    def kv_copy(exchange, source, target, peer, slot):
+        return pltpu.make_async_remote_copy(
+            src_ref=source,
+            dst_ref=target,
+            send_sem=kv_send.at[exchange, peer],
+            recv_sem=kv_recv.at[exchange, slot],
+            device_id={"kv": peer},
+            device_id_type=pl.DeviceIdType.MESH,
+        )
+
+    def kv_start(exchange, source_of, target):
+        def body(step, carry):
+            peer = lax.rem(me + step, n_kv)
+            kv_copy(exchange, source_of(peer), target.at[me], peer, me).start()
+            return carry
+
+        lax.fori_loop(1, n_kv, body, 0)
+
+    def kv_arrive(exchange, target):
+        def body(step, carry):
+            peer = lax.rem(me + step, n_kv)
+            kv_copy(exchange, target.at[peer], target.at[peer], peer, peer).wait_recv()
+            return carry
+
+        lax.fori_loop(1, n_kv, body, 0)
+
+    def kv_sent(exchange, source_of, target):
+        def body(step, carry):
+            peer = lax.rem(me + step, n_kv)
+            kv_copy(exchange, source_of(peer), target.at[me], peer, me).wait_send()
+            return carry
+
+        lax.fori_loop(1, n_kv, body, 0)
+
+    def tp_copy(index, source, target):
+        return pltpu.make_async_remote_copy(
+            src_ref=source,
+            dst_ref=target,
+            send_sem=tp_send.at[index],
+            recv_sem=tp_recv.at[index],
+            device_id={"tp": 1 - core},
+            device_id_type=pl.DeviceIdType.MESH,
+        )
+
+    def feed_forward(which, gathered, gain_ref, gate, up, down, partial, landed):
+        gather_id, scatter_id = ((GATHER_A, SCATTER_A), (GATHER_B, SCATTER_B))[which]
+        kv_start(gather_id, lambda peer: gathered.at[me], gathered)
+        for copy in (loads[0:2], loads[9:11])[which]:
+            copy.wait()
+        kv_arrive(gather_id, gathered)
+        wide = gathered[...].astype(f32).reshape(n_kv * ROW_PAD, width)
+        squares = jnp.sum(wide * wide, axis=1, keepdims=True)
+        squares_out[which] = jnp.broadcast_to(squares, squares_out.shape[1:])
+        scaled = (wide * gain_ref[...]).astype(bf16)
+        gate_part = jnp.dot(scaled, gate[...], preferred_element_type=f32)
+        gate_up_out[which, 0] = gate_part.astype(bf16)
+        copies = [
+            tp_copy(3 * which, squares_out.at[which], squares_in.at[which]),
+            tp_copy(3 * which + 1, gate_up_out.at[which, 0], gate_up_in.at[which, 0]),
+            tp_copy(3 * which + 2, gate_up_out.at[which, 1], gate_up_in.at[which, 1]),
+        ]
+        copies[0].start()
+        copies[1].start()
+        up_part = jnp.dot(scaled, up[...], preferred_element_type=f32)
+        gate_up_out[which, 1] = up_part.astype(bf16)
+        copies[2].start()
+        for copy in copies:
+            copy.wait_recv()
+        total = squares + squares_in[which][:, 0:1]
+        inverse = lax.rsqrt(total / model + EPSILON)
+        gate_sum = (gate_part + gate_up_in[which, 0].astype(f32)) * inverse
+        up_sum = (up_part + gate_up_in[which, 1].astype(f32)) * inverse
+        hidden = (gate_sum / (1.0 + jnp.exp(-gate_sum)) * up_sum).astype(bf16)
+        loads[(2, 11)[which]].wait()
+        branch = jnp.dot(hidden, down[...], preferred_element_type=f32)
+        partial[...] = branch.reshape(n_kv, ROW_PAD, width).astype(bf16)
+        landed[me] = partial[me]
+        kv_start(scatter_id, lambda peer: partial.at[peer], landed)
+        kv_arrive(scatter_id, landed)
+        for copy in copies:
+            copy.wait_send()
+        return jnp.sum(landed[...].astype(f32), axis=0)
+
+    branch_a = feed_forward(
+        0, gather_a, gain_pre_ref, gate_pre, up_pre, down_pre, partial_a, landed_a
+    )
+    stream_a = (residual_pad[...] + 0.5 * branch_a).astype(bf16)
+
+    stream_out[...] = stream_a
+    stream_copy = tp_copy(6, stream_out, stream_in)
+    stream_copy.start()
+    own = stream_a.astype(f32)
+    own_squares = jnp.sum(own * own, axis=1, keepdims=True)
+    stream_copy.wait_recv()
+    other = stream_in[...].astype(f32)
+    squares = own_squares + jnp.sum(other * other, axis=1, keepdims=True)
+    inverse = lax.rsqrt(squares / model + EPSILON)
+    own_scaled = (own * gain_mix_ref[core]).astype(bf16)
+    other_scaled = (other * gain_mix_ref[1 - core]).astype(bf16)
+    depth = column_out.shape[2]
+    half_blocks = n_kv // 2
+    for block in range(half_blocks):
+        span = slice(block * depth, (block + 1) * depth)
+        column_out[core * half_blocks + block] = own_scaled[:, span]
+        column_out[(1 - core) * half_blocks + block] = other_scaled[:, span]
+    column_in[me] = column_out[me]
+    kv_start(COLUMNS, lambda peer: column_out.at[peer], column_in)
+    kv_arrive(COLUMNS, column_in)
+    columns = column_in[...].astype(f32).reshape(n_kv * ROW_PAD, depth).astype(bf16)
+    for index in range(4):
+        loads[3 + index].wait()
+        product = jnp.dot(columns, proj_weights[index], preferred_element_type=f32)
+        proj_out[index] = product.reshape(n_kv, ROW_PAD, width).astype(bf16)
+        proj_in[index, me] = proj_out[index, me]
+        kv_start(
+            PROJECT + index,
+            lambda peer, index=index: proj_out.at[index, peer],
+            proj_in.at[index],
+        )
+
+    def projected(index):
+        kv_arrive(PROJECT + index, proj_in.at[index])
+        return jnp.sum(proj_in[index].astype(f32), axis=0) * inverse
+
+    heads = width // HEAD_DIM
+    floor_rate = lower_ref[...]
+    forget_pre = projected(0)
+    keep = floor_rate + (1.0 - floor_rate) / (1.0 + jnp.exp(-forget_pre))
+    inject = (1.0 - floor_rate) / (1.0 + jnp.exp(forget_pre))
+    for head in range(heads):
+        span = slice(head * HEAD_DIM, (head + 1) * HEAD_DIM)
+        keep_t[head] = keep[:, span].T
+        inject_t[head] = inject[:, span].T
+    value_pre = projected(1)
+    for head in range(heads):
+        span = slice(head * HEAD_DIM, (head + 1) * HEAD_DIM)
+        value_rows[head] = value_pre[:, span]
+    query_pre = projected(2)
+    query = query_pre / (1.0 + jnp.exp(-query_pre))
+    for head in range(heads):
+        span = slice(head * HEAD_DIM, (head + 1) * HEAD_DIM)
+        query_t[head] = query[:, span].T
+    loads[7].wait()
+
+    def recur(head, carry):
+        keep_cols = keep_t[head]
+        inject_cols = inject_t[head]
+        query_cols = query_t[head]
+        values = value_rows[head]
+        for row in range(rows):
+            col = slice(row, row + 1)
+            new = keep_cols[:, col] * state[row, head] + inject_cols[:, col] * values[col, :]
+            state[row, head] = new
+            readout[head, col, :] = jnp.sum(query_cols[:, col] * new, axis=0, keepdims=True)
+        return carry
+
+    lax.fori_loop(0, heads, recur, 0)
+    store = pltpu.make_async_copy(state, next_hbm, store_sem)
+    outgate_pre = projected(3)
+    store.start()
+    outgate = outgate_pre / (1.0 + jnp.exp(-outgate_pre))
+    mixed_heads = []
+    for head in range(heads):
+        span = slice(head * HEAD_DIM, (head + 1) * HEAD_DIM)
+        read = readout[head]
+        scale = lax.rsqrt(jnp.mean(read * read, axis=1, keepdims=True) + EPSILON)
+        mixed_heads.append(read * scale * head_gain_ref[:, span] * outgate[:, span])
+    mixed_rows = jnp.concatenate(mixed_heads, axis=1).astype(bf16)
+    loads[8].wait()
+    mixed_part = jnp.dot(mixed_rows, out_weight[...], preferred_element_type=f32)
+    mixed_out[0] = mixed_part[:, 0:width]
+    mixed_out[1] = mixed_part[:, width:model]
+    mixed_copy = tp_copy(7, mixed_out.at[1 - core], mixed_in)
+    mixed_copy.start()
+    mixed_copy.wait_recv()
+    mixed = mixed_out[core] + mixed_in[...]
+    stream_b = (stream_out[...].astype(f32) + mixed).astype(bf16)
+    gather_b[me] = stream_b
+    branch_b = feed_forward(
+        1, gather_b, gain_post_ref, gate_post, up_post, down_post, partial_b, landed_b
+    )
+    layer_out = (gather_b[me].astype(f32) + 0.5 * branch_b).astype(bf16)
+    layer_ref[...] = layer_out[0:rows, :]
+
+    stream_copy.wait_send()
+    mixed_copy.wait_send()
+    kv_sent(GATHER_A, lambda peer: gather_a.at[me], gather_a)
+    kv_sent(SCATTER_A, lambda peer: partial_a.at[peer], landed_a)
+    kv_sent(COLUMNS, lambda peer: column_out.at[peer], column_in)
+    for index in range(4):
+        kv_sent(
+            PROJECT + index,
+            lambda peer, index=index: proj_out.at[index, peer],
+            proj_in.at[index],
+        )
+    kv_sent(GATHER_B, lambda peer: gather_b.at[me], gather_b)
+    kv_sent(SCATTER_B, lambda peer: partial_b.at[peer], landed_b)
+    store.wait()
+
+
+def fused_shards(
+    n_kv,
+    residual_in,
+    gain_pre,
+    gate_pre,
+    up_pre,
+    down_pre,
+    gain_mix,
+    query_weight,
+    forget_weight,
+    value_weight,
+    outgate_weight,
+    lower_bound,
+    head_gain,
+    out_weight,
+    gain_post,
+    gate_post,
+    up_post,
+    down_post,
+    memory_state,
+):
+    rows, width = residual_in.shape
+    depth = query_weight.shape[0]
+    hidden = gate_pre.shape[1]
+    heads = width // HEAD_DIM
+    all_rows = n_kv * ROW_PAD
+    f32, bf16 = jnp.float32, jnp.bfloat16
+    vmem = pl.BlockSpec(memory_space=pltpu.VMEM)
+    hbm = pl.BlockSpec(memory_space=pl.ANY)
+    like = lambda array: pltpu.VMEM(array.shape, array.dtype)
+    blocks = lambda: pltpu.VMEM((n_kv, ROW_PAD, width), bf16)
+    return pl.pallas_call(
+        functools.partial(fused_layer, n_kv),
+        out_shape=(
+            jax.ShapeDtypeStruct(residual_in.shape, residual_in.dtype),
+            jax.ShapeDtypeStruct(memory_state.shape, memory_state.dtype),
+        ),
+        in_specs=[vmem] * 6 + [hbm] * 12,
+        out_specs=(vmem, hbm),
+        scratch_shapes=[
+            like(gate_pre),
+            like(up_pre),
+            like(down_pre),
+            pltpu.VMEM((4,) + query_weight.shape, bf16),
+            like(out_weight),
+            like(gate_post),
+            like(up_post),
+            like(down_post),
+            like(memory_state),
+            blocks(),
+            blocks(),
+            blocks(),
+            blocks(),
+            blocks(),
+            blocks(),
+            pltpu.VMEM((2, 2, all_rows, hidden), bf16),
+            pltpu.VMEM((2, 2, all_rows, hidden), bf16),
+            pltpu.VMEM((2, all_rows, 128), f32),
+            pltpu.VMEM((2, all_rows, 128), f32),
+            pltpu.VMEM((ROW_PAD, width), bf16),
+            pltpu.VMEM((ROW_PAD, width), bf16),
+            pltpu.VMEM((n_kv, ROW_PAD, depth), bf16),
+            pltpu.VMEM((n_kv, ROW_PAD, depth), bf16),
+            pltpu.VMEM((4, n_kv, ROW_PAD, width), bf16),
+            pltpu.VMEM((4, n_kv, ROW_PAD, width), bf16),
+            pltpu.VMEM((2, ROW_PAD, width), f32),
+            pltpu.VMEM((ROW_PAD, width), f32),
+            pltpu.VMEM((ROW_PAD, width), f32),
+            pltpu.VMEM((heads, HEAD_DIM, ROW_PAD), f32),
+            pltpu.VMEM((heads, HEAD_DIM, ROW_PAD), f32),
+            pltpu.VMEM((heads, HEAD_DIM, ROW_PAD), f32),
+            pltpu.VMEM((heads, ROW_PAD, HEAD_DIM), f32),
+            pltpu.VMEM((heads, ROW_PAD, HEAD_DIM), f32),
+            pltpu.SemaphoreType.DMA((12,)),
+            pltpu.SemaphoreType.DMA,
+            pltpu.SemaphoreType.DMA((KV_EXCHANGES, n_kv)),
+            pltpu.SemaphoreType.DMA((KV_EXCHANGES, n_kv)),
+            pltpu.SemaphoreType.DMA((8,)),
+            pltpu.SemaphoreType.DMA((8,)),
+        ],
+        compiler_params=pltpu.CompilerParams(
+            collective_id=0, has_side_effects=True, vmem_limit_bytes=60 * 1024 * 1024
+        ),
+    )(
+        residual_in,
+        gain_pre.reshape(1, width),
+        gain_mix.reshape(2, 1, width),
+        lower_bound.reshape(1, width),
+        head_gain.reshape(1, width),
+        gain_post.reshape(1, width),
+        gate_pre,
+        up_pre,
+        down_pre,
+        query_weight,
+        forget_weight,
+        value_weight,
+        outgate_weight,
+        out_weight,
+        gate_post,
+        up_post,
+        down_post,
+        memory_state,
+    )
+
+
 def solution(mesh):
+    n_kv, n_tp = mesh.shape["kv"], mesh.shape["tp"]
+    fits = n_tp == 2 and D % (128 * n_kv) == 0 and n_kv % 2 == 0
+    body = functools.partial(fused_shards, n_kv) if fits else shards
     in_specs = (
         P("kv", "tp"),
         P("tp"),
@@ -164,4 +591,4 @@
         P("kv", "tp", None, None),
     )
     out_specs = (P("kv", "tp"), P("kv", "tp", None, None))
-    return jax.shard_map(shards, mesh=mesh, in_specs=in_specs, out_specs=out_specs, check_vma=False)
+    return jax.shard_map(body, mesh=mesh, in_specs=in_specs, out_specs=out_specs, check_vma=False)

time: 354 us -> 91.1 us (0.26)
  blocking collectives: 211 us -> 0 us
  Pallas kernels: 0 us -> 77.9 us
  waiting for transfers between devices: 50.5 us -> 0 us
  starting transfers between devices: 48.1 us -> 0 us
  between operations: 15.6 us -> 0.66 us
  matrix products: 12.6 us -> 0 us
  other arithmetic: 8.58 us -> 0 us
  local copies, waits for them, and re-layouts: 4.76 us -> 12.2 us
    unnamed x5 -> x0, blocking collectives: 133 us -> none
    pallas_call x0 -> x1, Pallas kernels: none -> 77.9 us  [fused_shards(): pl.pallas_call(functools.partial(fused_layer, n_kv), out_shape=(jax.Shape...]
    all_gather x5 -> x0, blocking collectives: 77.6 us -> none  [the longest x2 72 us: channel_mixer(): gathered = lax.all_gather(row_block, 'kv', axis=0, tiled=True)]
    unnamed x12 -> x0, starting transfers between devices: 40.4 us -> none
    reduce_scatter x5 -> x0, waiting for transfers between devices: 38.2 us -> none  [the longest x2 22.2 us: channel_mixer(): lax.psum_scatter(up_part.astype(jnp.bfloat16), 'tp', scatter_dimension=0,...]
    dot_general x9 -> x0, matrix products: 12.6 us -> none  [the longest x2 3.86 us: channel_mixer(): gate_part = jnp.dot(scaled, gate_weight, preferred_element_type=jnp.float32)]
    unnamed x43 -> x10, local copies, waits for them, and re-layouts: 4.63 us -> 12.2 us
    all_to_all x1 -> x0, starting transfers between devices: 7.47 us -> none  [token_mixer(): lax.all_to_all(scaled, 'kv', split_axis=1, concat_axis=0, tiled=True)]
  transfers between devices with their start and end apart: 18 -> 0, of which waited for: 9 -> 0; matrix products, arithmetic and copies ran while one was open for 2% -> 0% of each run, Pallas kernels for 0% -> 0%
where the time goes in v1:
time: 91.1 us; the launch traced here: 90.8 us
  Pallas kernels  77.9 us (86%)
  local copies, waits for them, and re-layouts  12.2 us (13%)
    pallas_call x1, Pallas kernels, fused_shards(): pl.pallas_call(functools.partial(fused_layer, n_kv), out_shape=(jax.Shape...  77.9 us
    unnamed x10, local copies, waits for them, and re-layouts  12.2 us

profile of v1, /device:TPU:8, one launch (start us, length us, event | category | flops | bytes accessed | tf_op | source)
XLA Modules:
  0.0 90.8 jit_solution(10009651242009912256)
XLA Ops:
  0.6 0.0 copy-start.1
  0.6 0.0 copy-start
  0.7 2.4 %copy.20.gate_pre_hbm = bf16[1024,352]{1,0:T(8,128)(2,1)} copy(bf16[1024,352]{0,1:T(8,128)(2,1)} %param.20) | data formatting | bytes 1441792 | tf_op args[2]
  3.0 2.3 %copy.21.up_pre_hbm = bf16[1024,352]{1,0:T(8,128)(2,1)} copy(bf16[1024,352]{0,1:T(8,128)(2,1)} %param.21) | data formatting | bytes 1441792 | tf_op args[3]
  5.3 0.0 copy-done
  5.3 1.2 %copy.22.gate_post_hbm = bf16[1024,352]{1,0:T(8,128)(2,1)} copy(bf16[1024,352]{0,1:T(8,128)(2,1)S(1)} %copy-done) | data formatting | bytes 1441792 | tf_op args[14]
  6.4 0.0 copy-done.1
  6.4 1.2 %copy.23.up_post_hbm = bf16[1024,352]{1,0:T(8,128)(2,1)} copy(bf16[1024,352]{0,1:T(8,128)(2,1)S(1)} %copy-done.1) | data formatting | bytes 1441792 | tf_op args[15]
  7.6 77.9 %shard_map.185 = (bf16[6,1024]{1,0:T(8,128)(2,1)}, f32[6,8,128,128]{3,2,1,0:T(8,128)}) custom-call(bf16[6,1024]{1,0:T(8,128)(2,1)} %residual_ref.1, f32[1,1024]{1,0:T(1,128)} %bitcast.6, f32[2,1,1024]{2,1,0:T(1,128)} %bitcast.5, f32[1,1024]{1,0:T(1,128)} %bitcast.7, f32[1,1024]{1,0:T(1,128)} %bitcast.8, f32[1,1024]{1,0:T(1,128)} %bitcast.9, ...), custom_call_target="tpu_custom_call" | custom-call | tf_op jit(solution)/shard_map/pallas_call | solution.py:495
  85.5 1.3 %copy.26 = bf16[6,1024]{1,0:T(8,128)(2,1)} copy(bf16[6,1024]{1,0:T(8,128)(2,1)} %get-tuple-element.4) | data formatting | bytes 24576
  86.9 3.9 %copy.27 = f32[6,8,128,128]{3,2,1,0:T(8,128)} copy(f32[6,8,128,128]{3,2,1,0:T(8,128)} %get-tuple-element.5) | data formatting | bytes 6291456
Async XLA Ops:
  0.6 5.8 %copy-start.1 = (bf16[1024,352]{0,1:T(8,128)(2,1)S(1)}, bf16[1024,352]{0,1:T(8,128)(2,1)}, u32[]{:S(2)}) copy-start(bf16[1024,352]{0,1:T(8,128)(2,1)} %param.33) | copy-start | bytes 2162692
  0.6 4.6 %copy-start = (bf16[1024,352]{0,1:T(8,128)(2,1)S(1)}, bf16[1024,352]{0,1:T(8,128)(2,1)}, u32[]{:S(2)}) copy-start(bf16[1024,352]{0,1:T(8,128)(2,1)} %param.32) | copy-start | bytes 2162692

commit v2 on v1

--- a/solution.py
+++ b/solution.py
@@ -149,6 +149,12 @@
 ROW_PAD = 8
 GATHER_A, SCATTER_A, COLUMNS, PROJECT, GATHER_B, SCATTER_B = 0, 1, 2, 3, 7, 8
 KV_EXCHANGES = 9
+
+
+def dot_columns(rows, weight_columns):
+    return lax.dot_general(
+        rows, weight_columns, (((1,), (1,)), ((), ())), preferred_element_type=jnp.float32
+    )
 
 
 def fused_layer(
@@ -201,6 +207,7 @@
     mixed_out,
     mixed_in,
     residual_pad,
+    sums_pad,
     keep_t,
     inject_t,
     query_t,
@@ -243,6 +250,7 @@
     residual_pad[0:rows, :] = residual_ref[...].astype(f32)
     gather_a[me] = residual_pad[...].astype(bf16)
     readout[...] = jnp.zeros_like(readout)
+    sums_pad[...] = jnp.zeros_like(sums_pad)
 
     barrier = pltpu.get_barrier_semaphore()
 
@@ -315,7 +323,7 @@
         squares = jnp.sum(wide * wide, axis=1, keepdims=True)
         squares_out[which] = jnp.broadcast_to(squares, squares_out.shape[1:])
         scaled = (wide * gain_ref[...]).astype(bf16)
-        gate_part = jnp.dot(scaled, gate[...], preferred_element_type=f32)
+        gate_part = dot_columns(scaled, gate[...])
         gate_up_out[which, 0] = gate_part.astype(bf16)
         copies = [
             tp_copy(3 * which, squares_out.at[which], squares_in.at[which]),
@@ -324,7 +332,7 @@
         ]
         copies[0].start()
         copies[1].start()
-        up_part = jnp.dot(scaled, up[...], preferred_element_type=f32)
+        up_part = dot_columns(scaled, up[...])
         gate_up_out[which, 1] = up_part.astype(bf16)
         copies[2].start()
         for copy in copies:
@@ -336,13 +344,14 @@
         hidden = (gate_sum / (1.0 + jnp.exp(-gate_sum)) * up_sum).astype(bf16)
         loads[(2, 11)[which]].wait()
         branch = jnp.dot(hidden, down[...], preferred_element_type=f32)
-        partial[...] = branch.reshape(n_kv, ROW_PAD, width).astype(bf16)
+        partial[...] = branch.reshape(n_kv, ROW_PAD, width)[:, 0:rows, :].astype(bf16)
         landed[me] = partial[me]
         kv_start(scatter_id, lambda peer: partial.at[peer], landed)
         kv_arrive(scatter_id, landed)
         for copy in copies:
             copy.wait_send()
-        return jnp.sum(landed[...].astype(f32), axis=0)
+        sums_pad[4 + which, 0:rows, :] = jnp.sum(landed[...].astype(f32), axis=0)
+        return sums_pad[4 + which]
 
     branch_a = feed_forward(
         0, gather_a, gain_pre_ref, gate_pre, up_pre, down_pre, partial_a, landed_a
@@ -373,7 +382,7 @@
     for index in range(4):
         loads[3 + index].wait()
         product = jnp.dot(columns, proj_weights[index], preferred_element_type=f32)
-        proj_out[index] = product.reshape(n_kv, ROW_PAD, width).astype(bf16)
+        proj_out[index] = product.reshape(n_kv, ROW_PAD, width)[:, 0:rows, :].astype(bf16)
         proj_in[index, me] = proj_out[index, me]
         kv_start(
             PROJECT + index,
@@ -383,7 +392,8 @@
 
     def projected(index):
         kv_arrive(PROJECT + index, proj_in.at[index])
-        return jnp.sum(proj_in[index].astype(f32), axis=0) * inverse
+        sums_pad[index, 0:rows, :] = jnp.sum(proj_in[index].astype(f32), axis=0)
+        return sums_pad[index] * inverse
 
     heads = width // HEAD_DIM
     floor_rate = lower_ref[...]
@@ -491,7 +501,7 @@
     vmem = pl.BlockSpec(memory_space=pltpu.VMEM)
     hbm = pl.BlockSpec(memory_space=pl.ANY)
     like = lambda array: pltpu.VMEM(array.shape, array.dtype)
-    blocks = lambda: pltpu.VMEM((n_kv, ROW_PAD, width), bf16)
+    blocks = lambda count: pltpu.VMEM((n_kv, count, width), bf16)
     return pl.pallas_call(
         functools.partial(fused_layer, n_kv),
         out_shape=(
@@ -501,21 +511,21 @@
         in_specs=[vmem] * 6 + [hbm] * 12,
         out_specs=(vmem, hbm),
         scratch_shapes=[
-            like(gate_pre),
-            like(up_pre),
+            pltpu.VMEM((hidden, width), bf16),
+            pltpu.VMEM((hidden, width), bf16),
             like(down_pre),
             pltpu.VMEM((4,) + query_weight.shape, bf16),
             like(out_weight),
-            like(gate_post),
-            like(up_post),
+            pltpu.VMEM((hidden, width), bf16),
+            pltpu.VMEM((hidden, width), bf16),
             like(down_post),
             like(memory_state),
-            blocks(),
-            blocks(),
-            blocks(),
-            blocks(),
-            blocks(),
-            blocks(),
+            blocks(ROW_PAD),
+            blocks(ROW_PAD),
+            blocks(rows),
+            blocks(rows),
+            blocks(rows),
+            blocks(rows),
             pltpu.VMEM((2, 2, all_rows, hidden), bf16),
             pltpu.VMEM((2, 2, all_rows, hidden), bf16),
             pltpu.VMEM((2, all_rows, 128), f32),
@@ -524,11 +534,12 @@
             pltpu.VMEM((ROW_PAD, width), bf16),
             pltpu.VMEM((n_kv, ROW_PAD, depth), bf16),
             pltpu.VMEM((n_kv, ROW_PAD, depth), bf16),
-            pltpu.VMEM((4, n_kv, ROW_PAD, width), bf16),
-            pltpu.VMEM((4, n_kv, ROW_PAD, width), bf16),
+            pltpu.VMEM((4, n_kv, rows, width), bf16),
+            pltpu.VMEM((4, n_kv, rows, width), bf16),
             pltpu.VMEM((2, ROW_PAD, width), f32),
             pltpu.VMEM((ROW_PAD, width), f32),
             pltpu.VMEM((ROW_PAD, width), f32),
+            pltpu.VMEM((6, ROW_PAD, width), f32),
             pltpu.VMEM((heads, HEAD_DIM, ROW_PAD), f32),
             pltpu.VMEM((heads, HEAD_DIM, ROW_PAD), f32),
             pltpu.VMEM((heads, HEAD_DIM, ROW_PAD), f32),
@@ -551,16 +562,16 @@
         lower_bound.reshape(1, width),
         head_gain.reshape(1, width),
         gain_post.reshape(1, width),
-        gate_pre,
-        up_pre,
+        gate_pre.T,
+        up_pre.T,
         down_pre,
         query_weight,
         forget_weight,
         value_weight,
         outgate_weight,
         out_weight,
-        gate_post,
-        up_post,
+        gate_post.T,
+        up_post.T,
         down_post,
         memory_state,
     )

time: 91.1 us -> 84.7 us (0.930)
  local copies, waits for them, and re-layouts: 12.2 us -> 5.23 us
    unnamed x10 -> x2, local copies, waits for them, and re-layouts: 12.2 us -> 5.23 us
where the time goes in v2:
time: 84.7 us; the launch traced here: 84.4 us
  Pallas kernels  78.5 us (93%)
  local copies, waits for them, and re-layouts  5.23 us (6%)
    pallas_call x1, Pallas kernels, fused_shards(): pl.pallas_call(functools.partial(fused_layer, n_kv), out_shape=(jax.Shape...  78.5 us
    unnamed x2, local copies, waits for them, and re-layouts  5.23 us

profile of v2, /device:TPU:8, one launch (start us, length us, event | category | flops | bytes accessed | tf_op | source)
XLA Modules:
  0.0 84.4 jit_solution(13889449234545743682)
XLA Ops:
  0.6 78.5 %shard_map.185 = (bf16[6,1024]{1,0:T(8,128)(2,1)}, f32[6,8,128,128]{3,2,1,0:T(8,128)}) custom-call(bf16[6,1024]{1,0:T(8,128)(2,1)} %residual_ref.1, f32[1,1024]{1,0:T(1,128)} %bitcast.14, f32[2,1,1024]{2,1,0:T(1,128)} %bitcast.13, f32[1,1024]{1,0:T(1,128)} %bitcast.15, f32[1,1024]{1,0:T(1,128)} %bitcast.16, f32[1,1024]{1,0:T(1,128)} %bitcast.17, ...), custom_call_target="tpu_custom_call" | custom-call | tf_op jit(solution)/shard_map/pallas_call | solution.py:505
  79.1 1.3 %copy.22 = bf16[6,1024]{1,0:T(8,128)(2,1)} copy(bf16[6,1024]{1,0:T(8,128)(2,1)} %get-tuple-element.4) | data formatting | bytes 24576
  80.5 3.9 %copy.23 = f32[6,8,128,128]{3,2,1,0:T(8,128)} copy(f32[6,8,128,128]{3,2,1,0:T(8,128)} %get-tuple-element.5) | data formatting | bytes 6291456
